TPU v7x, 128 devices: a whole 4x4x4 slice. The times are simulated.
128 devices in a mesh: kv: 16 (over z, x), tp: 8 (over y, core).
Axes of the slice: x: 4, y: 4, z: 4, core: 2. Of those that a mesh axis runs over, the one named last changes fastest.
Arguments:
- tokens: bfloat16 [32768, 2048], P('kv'), may hold values from -6 to 6
- norm_gain: bfloat16 [2048], replicated, may hold values from 0.099609375 to 1.8984375
- query_weight: bfloat16 [2048, 1024], P(None, 'tp'), may hold values from -0.125 to 0.125
- cmp_key_weight: bfloat16 [2048, 512], P(None, 'tp'), may hold values from -0.125 to 0.125
- cmp_value_weight: bfloat16 [2048, 512], P(None, 'tp'), may hold values from -0.125 to 0.125
- sel_key_weight: bfloat16 [2048, 512], P(None, 'tp'), may hold values from -0.125 to 0.125
- sel_value_weight: bfloat16 [2048, 512], P(None, 'tp'), may hold values from -0.125 to 0.125
- branch_weight: bfloat16 [2, 2048, 16], replicated, may hold values from -0.125 to 0.125
- key_embed: bfloat16 [8, 32, 64], P('tp'), may hold values from -3 to 3
- key_inner: bfloat16 [8, 2048, 64], P('tp'), may hold values from -0.125 to 0.125
- key_outer: bfloat16 [8, 64, 64], P('tp'), may hold values from -0.75 to 0.75
- value_embed: bfloat16 [8, 32, 64], P('tp'), may hold values from -3 to 3
- value_inner: bfloat16 [8, 2048, 64], P('tp'), may hold values from -0.125 to 0.125
- value_outer: bfloat16 [8, 64, 64], P('tp'), may hold values from -0.75 to 0.75
- out_weight: bfloat16 [1024, 2048], replicated, may hold values from -0.1875 to 0.1875
- chosen: int32 [8, 256, 8], P('tp'), may hold values from 0 to 511, as said below
Outputs:
- attended: bfloat16 [32768, 2048], P(('kv', 'tp'))
Inputs may be any that keep to these rules, and one draw needn't show every extreme that they name: `chosen`: each entry is the index of a block of 64 positions in the whole sequence. For every key head and query block, its 8 entries lie in 8 different aligned spans of 2048 positions (at most one from any span), and none lies inside the query block's own positions.
All inputs are finite; a program needn't handle non-finite values.
Results may differ from a plain program's by a relative error of at most 0.0075.
Values may be sent and summed in bfloat16 or wider, within the bound.
No kernel may reach another device: no remote copies, remote signals or barrier semaphores. Data moves between devices by JAX's collectives and lax.ppermute only.
A program may use at most 128 MiB of HBM per device.

v0:
```python
import jax
import jax.numpy as jnp
from jax import lax
from jax.sharding import PartitionSpec as P

HEAD_DIM = 64
CMP_BLOCK = 32
SEL_BLOCK = 64
Q_BLOCK = 128
FAR_PICKS = 8
ROPE_BASE = 10000.0
norm_eps = 1e-06
masked_score = -1000000000.0


def copy_for_each(x, axis):
    peers = lax.axis_size(axis)
    return lax.all_to_all(jnp.broadcast_to(x[None], (peers, *x.shape)), axis, 0, 0, tiled=True)


def in_order(pieces, dim):
    shape = list(pieces.shape[1:])
    shape[dim] *= pieces.shape[0]
    return jnp.moveaxis(pieces, 0, dim).reshape(shape)


def collect(x, axis, dim):
    pieces = copy_for_each(x, axis)
    return in_order(pieces, dim)


def rotate(values_in, positions):
    half_dim = values_in.shape[-1] // 2
    inverse = ROPE_BASE ** (-jnp.arange(half_dim, dtype=jnp.float32) / half_dim)
    rotary_phases = positions.astype(jnp.float32)[:, None] * inverse[None, :]
    cosine = jnp.cos(rotary_phases)[:, None, :]
    sine = jnp.sin(rotary_phases)[:, None, :]
    first_half = values_in[..., :half_dim]
    second_half = values_in[..., half_dim:]
    return jnp.concatenate(
        [first_half * cosine - second_half * sine, second_half * cosine + first_half * sine],
        axis=-1,
    )


def summarize(raw_rows, embed, inner, outer):
    kv_local = embed.shape[0]
    block_count = raw_rows.shape[0] // CMP_BLOCK
    blocked = (
        raw_rows.reshape(block_count, CMP_BLOCK, kv_local, HEAD_DIM)
        .transpose(2, 0, 1, 3)
        .astype(jnp.float32)
    )
    blocked = (blocked + embed.astype(jnp.float32)[:, None]).astype(jnp.bfloat16)
    blocked = blocked.reshape(kv_local, block_count, CMP_BLOCK * HEAD_DIM)
    hidden = jax.nn.gelu(
        jnp.einsum("knc,kce->kne", blocked, inner, preferred_element_type=jnp.float32)
    ).astype(jnp.bfloat16)
    return jnp.einsum("kne,kef->knf", hidden, outer, preferred_element_type=jnp.float32).astype(
        jnp.bfloat16
    )


def per_device(
    tokens,
    norm_gain,
    query_weight,
    cmp_key_weight,
    cmp_value_weight,
    sel_key_weight,
    sel_value_weight,
    branch_weight,
    key_embed,
    key_inner,
    key_outer,
    value_embed,
    value_inner,
    value_outer,
    out_weight,
    chosen,
):
    tok_rows = tokens.shape[0]
    kv_local = key_embed.shape[0]
    heads_local = query_weight.shape[1] // HEAD_DIM
    group_size = heads_local // kv_local
    owners = lax.axis_size("kv")
    dev_index = lax.axis_index("kv")
    offset = dev_index * tok_rows
    positions = offset + jnp.arange(tok_rows, dtype=jnp.int32)
    scale = HEAD_DIM ** (-0.5)
    expanded_mask = tokens.astype(jnp.float32)
    normed = (
        expanded_mask
        * lax.rsqrt(jnp.mean(expanded_mask * expanded_mask, axis=-1, keepdims=True) + norm_eps)
        * norm_gain.astype(jnp.float32)
    ).astype(jnp.bfloat16)
    gate_cols = lax.dynamic_slice_in_dim(
        branch_weight, lax.axis_index("tp") * heads_local, heads_local, 2
    )
    q_width = heads_local * HEAD_DIM
    kv_width = kv_local * HEAD_DIM
    joined_weight = jnp.concatenate(
        [
            query_weight,
            cmp_key_weight,
            cmp_value_weight,
            sel_key_weight,
            sel_value_weight,
            gate_cols[0],
            gate_cols[1],
        ],
        axis=1,
    )
    projected = jnp.dot(normed, joined_weight, preferred_element_type=jnp.float32)
    bounds = [
        q_width,
        q_width + kv_width,
        q_width + 2 * kv_width,
        q_width + 3 * kv_width,
        q_width + 4 * kv_width,
        q_width + 4 * kv_width + heads_local,
    ]
    (
        query_part,
        cmp_key_part,
        cmp_value_part,
        sel_key_part,
        sel_value_part,
        gate_cmp_part,
        gate_sel_part,
    ) = jnp.split(projected, bounds, axis=1)
    query = query_part.reshape(tok_rows, heads_local, HEAD_DIM)
    q_plain = query.astype(jnp.bfloat16)
    q_turn = rotate(query, positions).astype(jnp.bfloat16)
    cmp_key = cmp_key_part.astype(jnp.bfloat16).reshape(tok_rows, kv_local, HEAD_DIM)
    cmp_value = cmp_value_part.astype(jnp.bfloat16).reshape(tok_rows, kv_local, HEAD_DIM)
    sel_key = rotate(sel_key_part.reshape(tok_rows, kv_local, HEAD_DIM), positions).astype(
        jnp.bfloat16
    )
    selected_value = sel_value_part.astype(jnp.bfloat16).reshape(tok_rows, kv_local, HEAD_DIM)
    gate_cmp = jax.nn.sigmoid(gate_cmp_part)
    gate_sel = jax.nn.sigmoid(gate_sel_part)
    summary = jnp.concatenate(
        [
            summarize(cmp_key, key_embed, key_inner, key_outer),
            summarize(cmp_value, value_embed, value_inner, value_outer),
        ],
        axis=-1,
    )
    summaries = collect(summary, "kv", 1)
    summary_count = summaries.shape[1]
    block_end = (jnp.arange(summary_count, dtype=jnp.int32) + 1) * CMP_BLOCK - 1
    q_group = q_plain.reshape(tok_rows, kv_local, group_size, HEAD_DIM).transpose(1, 0, 2, 3)
    cmp_scores = (
        jnp.einsum(
            "ktgd,kcd->ktgc", q_group, summaries[..., :HEAD_DIM], preferred_element_type=jnp.float32
        )
        * scale
    )
    usable = (block_end[None, :] <= positions[:, None])[None, :, None, :]
    cmp_probs = jax.nn.softmax(
        jnp.where(usable, cmp_scores, masked_score), axis=-1
    ) * usable.astype(jnp.float32)
    out_cmp = jnp.einsum(
        "ktgc,kcd->ktgd",
        cmp_probs.astype(jnp.bfloat16),
        summaries[..., HEAD_DIM:],
        preferred_element_type=jnp.float32,
    )
    out_cmp = out_cmp.transpose(1, 0, 2, 3).reshape(tok_rows, heads_local, HEAD_DIM)
    span_queries = tok_rows // Q_BLOCK
    span_blocks = tok_rows // SEL_BLOCK
    kv_sel = jnp.concatenate([sel_key, selected_value], axis=-1).transpose(1, 0, 2)
    all_picks = chosen.reshape(kv_local, owners, span_queries, FAR_PICKS)
    my_picks = lax.dynamic_index_in_dim(all_picks, dev_index, 1, keepdims=False)
    head_lane = jnp.arange(kv_local, dtype=jnp.int32)[:, None, None]
    matches = all_picks // span_blocks == dev_index
    wanted = jnp.sum(jnp.where(matches, all_picks % span_blocks, 0), axis=3)
    blocked = kv_sel.reshape(kv_local, span_blocks, SEL_BLOCK, 2 * HEAD_DIM)
    outgoing = blocked[head_lane, wanted]
    incoming = lax.all_to_all(outgoing, "kv", split_axis=1, concat_axis=1, tiled=True)
    source = my_picks // span_blocks
    query_lane = jnp.arange(span_queries, dtype=jnp.int32)[None, :, None]
    picked = incoming[head_lane, source, query_lane]
    own_keys = kv_sel.reshape(kv_local, span_queries, Q_BLOCK, 2 * HEAD_DIM)
    keys_all = jnp.concatenate(
        [own_keys, picked.reshape(kv_local, span_queries, FAR_PICKS * SEL_BLOCK, 2 * HEAD_DIM)],
        axis=2,
    )
    query_pos = positions.reshape(span_queries, Q_BLOCK)
    far_pos = (my_picks[..., None] * SEL_BLOCK + jnp.arange(SEL_BLOCK, dtype=jnp.int32)).reshape(
        kv_local, span_queries, FAR_PICKS * SEL_BLOCK
    )
    key_pos = jnp.concatenate([query_pos[None], far_pos], axis=2)
    q_sel = q_turn.reshape(span_queries, Q_BLOCK, kv_local, group_size, HEAD_DIM).transpose(
        2, 0, 1, 3, 4
    )
    sel_scores = (
        jnp.einsum(
            "knqgd,knmd->knqgm", q_sel, keys_all[..., :HEAD_DIM], preferred_element_type=jnp.float32
        )
        * scale
    )
    allowed_keys = key_pos[:, :, None, None, :] <= query_pos[None, :, :, None, None]
    sel_probs = jax.nn.softmax(jnp.where(allowed_keys, sel_scores, masked_score), axis=-1)
    out_sel = jnp.einsum(
        "knqgm,knmd->knqgd",
        sel_probs.astype(jnp.bfloat16),
        keys_all[..., HEAD_DIM:],
        preferred_element_type=jnp.float32,
    )
    out_sel = out_sel.transpose(1, 2, 0, 3, 4).reshape(tok_rows, heads_local, HEAD_DIM)
    mixed = (
        (gate_cmp[..., None] * out_cmp + gate_sel[..., None] * out_sel)
        .reshape(tok_rows, heads_local * HEAD_DIM)
        .astype(jnp.bfloat16)
    )
    head_rows = lax.all_to_all(mixed, "tp", split_axis=0, concat_axis=1, tiled=True)
    return jnp.dot(head_rows, out_weight, preferred_element_type=jnp.float32).astype(jnp.bfloat16)


def solution(mesh):
    placed = (
        P("kv", None),
        P(),
        P(None, "tp"),
        P(None, "tp"),
        P(None, "tp"),
        P(None, "tp"),
        P(None, "tp"),
        P(),
        P("tp", None, None),
        P("tp", None, None),
        P("tp", None, None),
        P("tp", None, None),
        P("tp", None, None),
        P("tp", None, None),
        P(),
        P("tp", None, None),
    )
    return jax.shard_map(
        per_device, mesh=mesh, in_specs=placed, out_specs=P(("kv", "tp"), None), check_vma=False
    )
```

profile of v0, /device:TPU:1, one launch (start us, length us, event | category | flops | bytes accessed | tf_op | source)
XLA Modules:
  0.0 171.9 jit_solution(5051237416359795915)
XLA Ops:
  0.8 5.1 %fusion.2 = f32[2048]{0:T(1024)S(1)} fusion(bf16[2048,2048]{1,0:T(8,128)(2,1)} %param.16), kind=kLoop, calls=%fused_computation.6 | loop fusion | flops 12580864 | bytes 8396800 | tf_op jit(solution)/shard_map/reduce_sum | solution.py:94
  12.4 5.5 %concatenate.68 = bf16[2048,388]{1,0:T(8,128)(2,1)} concatenate(bf16[2048,128]{1,0:T(8,128)(2,1)} %param.18, bf16[2048,64]{1,0:T(8,128)(2,1)} %copy.58, bf16[2048,64]{1,0:T(8,128)(2,1)} %copy.59, bf16[2048,64]{1,0:T(8,128)(2,1)} %copy.60, bf16[2048,64]{1,0:T(8,128)(2,1)} %copy.61, bf16[2048,2]{1,0:T(8,128)(2,1)S(1)} %copy.62, bf16[2048,2]{1,0:T(8,128)(2,1)S(1)} %copy.63), dimensions={1} | concatenate | bytes 3178496 | tf_op jit(solution)/shard_map/concatenate | solution.py:102
  17.8 9.4 %fusion.119 = (bf16[2048,388]{0,1:T(8,128)(2,1)S(1)}, f32[2048,388]{0,1:T(8,128)}) fusion(bf16[2048,388]{1,0:T(8,128)(2,1)} %concatenate.68, bf16[2048,2048]{1,0:T(8,128)(2,1)} %param.16, f32[2048]{0:T(1024)S(1)} %convert_element_type.126, f32[2048]{0:T(1024)S(1)} %add_rsqrt_fusion), kind=kOutput, calls=%fused_computation.179 | convolution fusion | flops 3272351744 | bytes 14761984 | tf_op jit(solution)/shard_map/dot_general | solution.py:114
  27.4 1.0 copy-done.11
  31.5 8.5 %all-to-all-start = ((bf16[16,1,64,128]{3,2,1,0:T(8,128)(2,1)}), bf16[16,1,64,128]{3,2,1,0:T(8,128)(2,1)}, u32[]{:S(2)}, u32[]{:S(2)}) async-start(bf16[16,1,64,128]{3,2,1,0:T(8,128)(2,1)} %broadcast_in_dim.34), calls=%async_computation | async-start | bytes 524288 | tf_op jit(solution)/shard_map/all_to_all | solution.py:18
  40.2 1.7 %slice_bitcast_fusion.14 = (bf16[8,8,16,128]{3,1,2,0:T(8,128)(2,1)}, bf16[2048,64]{0,1:T(8,128)(2,1)S(1)}) fusion(bf16[2048,388]{0,1:T(8,128)(2,1)} %copy-done.11), kind=kLoop, calls=%fused_computation.176 | loop fusion | bytes 786432
  41.9 1.6 fusion.78
  43.5 1.1 slice_bitcast_fusion.4
  44.5 1.3 split.34
  46.7 1.8 %multiply_cosine_fusion.1 = (f32[2048,32]{0,1:T(8,128)}, f32[2048,32]{0,1:T(8,128)}) fusion(f32[32]{0:T(128)S(1)} %multiply_power_fusion, f32[2048]{0:T(1024)S(1)} %get-tuple-element.30), kind=kLoop, calls=%fused_computation.56 | loop fusion | flops 65536 | bytes 532608 | tf_op jit(solution)/shard_map/cos | solution.py:36
  48.5 1.1 fusion.35
  50.3 1.8 %broadcast_compare_fusion.1 = pred[16,128,640]{2,1,0:T(8,128)(4,1)} fusion(s32[16,128]{1,0:T(8,128)S(1)} %add_add_fusion, s32[16,640]{1,0:T(8,128)S(1)} %add_bitcast_fusion), kind=kLoop, calls=%fused_computation.30 | loop fusion | flops 1310720 | bytes 1359872 | tf_op jit(solution)/shard_map/le | solution.py:204
  52.5 3.1 %gather_fusion = bf16[256,64,128]{2,1,0:T(8,128)(2,1)} fusion(bf16[1,32,64,128]{3,2,1,0:T(8,128)(2,1)S(1)} %pad_maximum_fusion.1, s32[256]{0:T(256)S(1)} %reshape.731), kind=kCustom, calls=%fused_computation | custom fusion | bytes 8390656 | tf_op jit(solution)/shard_map/gather | solution.py:180
  55.8 6.8 %all-to-all-start.1 = ((bf16[1,16,16,64,128]{4,3,2,0,1:T(8,128)(2,1)}), bf16[1,16,16,64,128]{4,3,2,0,1:T(8,128)(2,1)}, u32[]{:S(2)}, u32[]{:S(2)}) async-start(bf16[1,16,16,64,128]{4,3,2,0,1:T(8,128)(2,1)} %bitcast.158), calls=%async_computation.1 | async-start | bytes 8388608 | tf_op jit(solution)/shard_map/all_to_all | solution.py:181
  62.6 2.1 %split.57 = bf16[2048,128]{0,1:T(8,128)(2,1)} slice(f32[2048,388]{0,1:T(8,128)} %get-tuple-element.24), slice={[0:2048], [0:128]} | slice | bytes 1048576 | tf_op jit(solution)/shard_map/split | solution.py:131
  68.5 4.2 %fusion.118 = (f32[2048,1024]{0,1:T(8,128)}, pred[2048,1024]{0,1:T(8,128)(4,1)S(1)}) fusion(s32[2048]{0:T(1024)S(1)} %get-tuple-element.29, s32[1024]{0:T(1024)S(1)} %multiply_add_fusion), kind=kLoop, calls=%fused_computation.178 | loop fusion | flops 4194304 | bytes 10498048 | tf_op jit(solution)/shard_map/convert_element_type | solution.py:163
  72.6 10.6 %fusion.121 = (f32[2048,2]{0,1:T(2,128)S(1)}, f32[2048,2,1024]{0,2,1:T(8,128)}) fusion(pred[2048,1024]{0,1:T(8,128)(4,1)S(1)} %get-tuple-element.20, bf16[2048,2,64]{0,2,1:T(8,128)(2,1)} %bitcast.173, bf16[1,1024,128]{2,1,0:T(8,128)(2,1)} %bitcast.14), kind=kOutput, calls=%fused_computation.181 | convolution fusion | flops 553649152 | bytes 19677184 | tf_op jit(solution)/shard_map/sub | solution.py:161
  83.3 9.4 %fusion.19 = f32[2048,2,64]{0,2,1:T(8,128)S(1)} fusion(f32[2048,2,1024]{0,2,1:T(8,128)} %get-tuple-element.28, f32[2048,1024]{0,1:T(8,128)} %get-tuple-element.19, f32[2048,2]{0,1:T(2,128)S(1)} %get-tuple-element.27, f32[2048,2]{0,1:T(2,128)S(1)} %copy-done.20, bf16[1,1024,128]{2,1,0:T(8,128)(2,1)} %bitcast.14), kind=kOutput, calls=%fused_computation.32 | convolution fusion | flops 549715968 | bytes 26509312 | tf_op jit(solution)/shard_map/ktgc,kcd->ktgd/dot_general | solution.py:164
  92.7 1.3 copy.96
  94.0 29.5 %all-to-all-done.1 = bf16[1,16,16,64,128]{4,3,2,0,1:T(8,128)(2,1)} async-done(((bf16[1,16,16,64,128]{4,3,2,0,1:T(8,128)(2,1)}), bf16[1,16,16,64,128]{4,3,2,0,1:T(8,128)(2,1)}, u32[]{:S(2)}, u32[]{:S(2)}) %all-to-all-start.1) | async-done | bytes 4194336 | tf_op jit(solution)/shard_map/all_to_all | solution.py:181
  123.5 4.5 %gather_fusion.1 = bf16[128,64,128]{2,1,0:T(8,128)(2,1)} fusion(bf16[1,16,16,64,128]{4,3,2,1,0:T(8,128)(2,1)} %bitcast.29, s32[128]{0:T(128)S(1)} %reshape.739), kind=kCustom, calls=%fused_computation.1 | custom fusion | bytes 4195840 | tf_op jit(solution)/shard_map/gather | solution.py:184
  127.9 2.9 %copy.83 = bf16[1,16,512,128]{2,3,1,0:T(8,128)(2,1)S(1)} copy(bf16[1,16,512,128]{3,2,1,0:T(8,128)(2,1)} %bitcast.159) | data formatting | bytes 4194304 | tf_op jit(solution)/shard_map/reshape | solution.py:187
  130.9 1.3 pad_maximum_fusion
  132.2 1.6 copy-done.2
  133.8 1.6 fusion.22
  135.4 7.2 %fusion.120 = (f32[16,128,2]{1,2,0:T(2,128)S(1)}, f32[16,128,2,640]{3,1,2,0:T(8,128)}) fusion(f32[16,128,2,640]{3,1,2,0:T(8,128)S(1)} %fusion.22, pred[16,128,640]{2,1,0:T(8,128)(4,1)S(1)} %copy-done.5), kind=kOutput, calls=%fused_computation.180 | output fusion | flops 15729279 | bytes 22298624 | tf_op jit(solution)/shard_map/sub | solution.py:205
  142.5 5.4 %fusion.18 = f32[16,128,2,64]{1,3,2,0:T(8,128)S(1)} fusion(f32[16,128,2,640]{3,1,2,0:T(8,128)} %get-tuple-element.26, f32[16,128,2]{1,2,0:T(2,128)S(1)} %get-tuple-element.25, bf16[1,16,640,128]{2,3,1,0:T(8,128)(2,1)S(1)} %copy-done.3), kind=kOutput, calls=%fused_computation.27 | convolution fusion | flops 340787200 | bytes 12861440 | tf_op jit(solution)/shard_map/knqgm,knmd->knqgd/dot_general | solution.py:206
  148.0 1.6 copy.84
  149.5 2.5 %reshape_transpose.10 = f32[8,256,128]{1,0,2:T(8,128)} reshape(f32[16,128,2,64]{1,0,3,2:T(8,128)} %copy.84) | data formatting | bytes 2097152 | tf_op jit(solution)/shard_map/reshape;transpose | solution.py:212
  152.1 1.6 fusion.26
  153.7 15.9 %all_to_all.26 = bf16[8,256,128]{1,2,0:T(8,128)(2,1)S(1)} all-to-all(bf16[8,256,128]{1,2,0:T(8,128)(2,1)S(1)} %copy.85), channel_id=1, replica_groups=mesh['kv'=16,'tp'=8] {'tp'}, dimensions={0} | all-to-all | bytes 1048576 | tf_op jit(solution)/shard_map/all_to_all | solution.py:218
  169.6 2.2 %convolution_convert_fusion = bf16[256,2048]{1,0:T(8,128)(2,1)} fusion(bf16[256,1024]{0,1:T(8,128)(2,1)S(1)} %bitcast.174, bf16[1024,2048]{1,0:T(8,128)(2,1)S(1)} %copy-done.23), kind=kOutput, calls=%fused_computation.31 | convolution fusion | flops 1074266112 | bytes 5767168 | tf_op jit(solution)/shard_map/dot_general | solution.py:219
  (114 shorter events, 16.4 us)
Async XLA Ops:
  0.0 29.9 %copy-start = (bf16[1,2048,64]{1,2,0:T(8,128)(2,1)S(1)}, bf16[1,2048,64]{1,2,0:T(8,128)(2,1)}, u32[]{:S(2)}) copy-start(bf16[1,2048,64]{1,2,0:T(8,128)(2,1)} %param.25) | copy-start | bytes 786436
  0.0 5.9 %copy-start.21 = (bf16[1,32,64]{2,1,0:T(8,128)(2,1)S(1)}, bf16[1,32,64]{2,1,0:T(8,128)(2,1)}, u32[]{:S(2)}) copy-start(bf16[1,32,64]{2,1,0:T(8,128)(2,1)} %param.24) | copy-start | bytes 12292
  0.0 6.0 %copy-start.22 = (bf16[1,32,64]{2,1,0:T(8,128)(2,1)S(1)}, bf16[1,32,64]{2,1,0:T(8,128)(2,1)}, u32[]{:S(2)}) copy-start(bf16[1,32,64]{2,1,0:T(8,128)(2,1)} %param.27) | copy-start | bytes 12292
  0.0 7.4 %copy-start.12 = (bf16[2048,64]{0,1:T(8,128)(2,1)S(1)}, bf16[2048,64]{0,1:T(8,128)(2,1)}, u32[]{:S(2)}) copy-start(bf16[2048,64]{0,1:T(8,128)(2,1)} %param.19) | copy-start | bytes 786436
  0.0 8.4 %copy-start.13 = (bf16[2048,64]{0,1:T(8,128)(2,1)S(1)}, bf16[2048,64]{0,1:T(8,128)(2,1)}, u32[]{:S(2)}) copy-start(bf16[2048,64]{0,1:T(8,128)(2,1)} %param.20) | copy-start | bytes 786436
  0.8 8.7 %copy-start.14 = (bf16[2048,64]{0,1:T(8,128)(2,1)S(1)}, bf16[2048,64]{0,1:T(8,128)(2,1)}, u32[]{:S(2)}) copy-start(bf16[2048,64]{0,1:T(8,128)(2,1)} %param.21) | copy-start | bytes 786436
  0.8 9.7 %copy-start.15 = (bf16[2048,64]{0,1:T(8,128)(2,1)S(1)}, bf16[2048,64]{0,1:T(8,128)(2,1)}, u32[]{:S(2)}) copy-start(bf16[2048,64]{0,1:T(8,128)(2,1)} %param.22) | copy-start | bytes 786436
  27.2 1.2 copy-start.11
  27.2 2.7 %copy-start.18 = (bf16[1,64,64]{2,1,0:T(8,128)(2,1)S(1)}, bf16[1,64,64]{2,1,0:T(8,128)(2,1)}, u32[]{:S(2)}) copy-start(bf16[1,64,64]{2,1,0:T(8,128)(2,1)} %param.26) | copy-start | bytes 24580
  27.2 3.0 %copy-start.16 = (bf16[1,2048,64]{1,2,0:T(8,128)(2,1)S(1)}, bf16[1,2048,64]{1,2,0:T(8,128)(2,1)}, u32[]{:S(2)}) copy-start(bf16[1,2048,64]{1,2,0:T(8,128)(2,1)} %param.28) | copy-start | bytes 786436
  27.2 3.1 %copy-start.19 = (bf16[1,64,64]{2,1,0:T(8,128)(2,1)S(1)}, bf16[1,64,64]{2,1,0:T(8,128)(2,1)}, u32[]{:S(2)}) copy-start(bf16[1,64,64]{2,1,0:T(8,128)(2,1)} %param.29) | copy-start | bytes 24580
  27.2 12.8 %copy-start.17 = (s32[1,256,8]{1,2,0:T(8,128)S(1)}, s32[1,256,8]{1,2,0:T(8,128)}, u32[]{:S(2)}) copy-start(s32[1,256,8]{1,2,0:T(8,128)} %param.31) | copy-start | bytes 24580
  31.5 24.3 %all-to-all-start = ((bf16[16,1,64,128]{3,2,1,0:T(8,128)(2,1)}), bf16[16,1,64,128]{3,2,1,0:T(8,128)(2,1)}, u32[]{:S(2)}, u32[]{:S(2)}) async-start(bf16[16,1,64,128]{3,2,1,0:T(8,128)(2,1)} %broadcast_in_dim.34), calls=%async_computation | async-start | bytes 524288 | tf_op jit(solution)/shard_map/all_to_all | solution.py:18
  52.5 3.1 %copy-start.9 = (f32[2048,32]{0,1:T(8,128)S(1)}, f32[2048,32]{0,1:T(8,128)}, u32[]{:S(2)}) copy-start(f32[2048,32]{0,1:T(8,128)} %get-tuple-element.21) | copy-start | bytes 786436
  52.5 3.1 %copy-start.10 = (f32[2048,32]{0,1:T(8,128)S(1)}, f32[2048,32]{0,1:T(8,128)}, u32[]{:S(2)}) copy-start(f32[2048,32]{0,1:T(8,128)} %get-tuple-element.22) | copy-start | bytes 786436
  55.8 9.1 %copy-start.6 = (bf16[8,8,16,128]{3,1,2,0:T(8,128)(2,1)S(1)}, bf16[8,8,16,128]{3,1,2,0:T(8,128)(2,1)}, u32[]{:S(2)}) copy-start(bf16[8,8,16,128]{3,1,2,0:T(8,128)(2,1)} %get-tuple-element.11) | copy-start | bytes 786436
  55.8 67.7 %all-to-all-start.1 = ((bf16[1,16,16,64,128]{4,3,2,0,1:T(8,128)(2,1)}), bf16[1,16,16,64,128]{4,3,2,0,1:T(8,128)(2,1)}, u32[]{:S(2)}, u32[]{:S(2)}) async-start(bf16[1,16,16,64,128]{4,3,2,0,1:T(8,128)(2,1)} %bitcast.158), calls=%async_computation.1 | async-start | bytes 8388608 | tf_op jit(solution)/shard_map/all_to_all | solution.py:181
  72.6 10.6 %copy-start.20 = (f32[2048,2]{0,1:T(2,128)S(1)}, f32[2048,2]{0,1:T(2,128)}, u32[]{:S(2)}) copy-start(f32[2048,2]{0,1:T(2,128)} %get-tuple-element.7) | copy-start | bytes 49156
  127.9 5.8 %copy-start.7 = (bf16[2,4,16,8,128]{4,3,1,0,2:T(8,128)(2,1)S(1)}, bf16[2,4,16,8,128]{4,3,1,0,2:T(8,128)(2,1)}, u32[]{:S(2)}) copy-start(bf16[2,4,16,8,128]{4,3,1,0,2:T(8,128)(2,1)} %copy.104) | copy-start | bytes 786436
  130.8 2.9 %copy-start.8 = (bf16[2,4,16,8,128]{4,3,1,0,2:T(8,128)(2,1)S(1)}, bf16[2,4,16,8,128]{4,3,1,0,2:T(8,128)(2,1)}, u32[]{:S(2)}) copy-start(bf16[2,4,16,8,128]{4,3,1,0,2:T(8,128)(2,1)} %copy.103) | copy-start | bytes 786436
  132.2 1.6 copy-start.2
  133.8 1.6 copy-start.5
  135.3 7.2 %copy-start.3 = (bf16[1,16,640,128]{2,3,1,0:T(8,128)(2,1)S(1)}, bf16[1,16,640,128]{2,3,1,0:T(8,128)(2,1)}, u32[]{:S(2)}) copy-start(bf16[1,16,640,128]{2,3,1,0:T(8,128)(2,1)} %copy-done.2) | copy-start | bytes 7864324
  142.5 9.5 %copy-start.4 = (f32[16,8,8,256]{3,2,1,0:T(8,128)S(1)}, f32[16,8,8,256]{3,2,1,0:T(8,128)}, u32[]{:S(2)}) copy-start(f32[16,8,8,256]{3,2,1,0:T(8,128)} %copy.96) | copy-start | bytes 3145732
  152.1 17.6 %copy-start.23 = (bf16[1024,2048]{1,0:T(8,128)(2,1)S(1)}, bf16[1024,2048]{1,0:T(8,128)(2,1)}, u32[]{:S(2)}) copy-start(bf16[1024,2048]{1,0:T(8,128)(2,1)} %param.30) | copy-start | bytes 12582916
  152.1 19.8 %copy-start.1 = (bf16[1,2048,64]{1,2,0:T(8,128)(2,1)S(1)}, bf16[1,2048,64]{1,2,0:T(8,128)(2,1)}, u32[]{:S(2)}) copy-start(bf16[1,2048,64]{1,2,0:T(8,128)(2,1)} %param.25) | copy-start | bytes 786436
where the time goes:
time: 173 us; the launch traced here: 172 us
  local copies, waits for them, and re-layouts  44 us (25%)
  matrix products  39.3 us (23%)
  waiting for transfers between devices  29.5 us (17%)
  other arithmetic  27.4 us (16%)
  blocking collectives  15.9 us (9%)
  starting transfers between devices  15.3 us (9%)
    all_to_all x1, waiting for transfers between devices, per_device(): lax.all_to_all(outgoing, 'kv', split_axis=1, concat_axis=1, tiled=True)  29.5 us
    all_to_all x1, blocking collectives, per_device(): lax.all_to_all(mixed, 'tp', split_axis=0, concat_axis=1, tiled=True)  15.9 us
    sub x1, matrix products, per_device(): jax.nn.softmax(jnp.where(usable, cmp_scores, masked_score), axis=-1)  10.6 us
    unnamed x58, local copies, waits for them, and re-layouts  10.2 us
    dot_general x1, matrix products, per_device(): jnp.einsum('ktgc,kcd->ktgd', cmp_probs.astype(jnp.bfloat16), summaries[.....  9.4 us
    dot_general x1, matrix products, per_device(): jnp.dot(normed, joined_weight, preferred_element_type=jnp.float32)  9.36 us
    all_to_all x1, starting transfers between devices, copy_for_each(): lax.all_to_all(jnp.broadcast_to(x[None], (peers, *x.shape)), axis, 0, 0,...  8.48 us
    sub x1, other arithmetic, per_device(): jax.nn.softmax(jnp.where(allowed_keys, sel_scores, masked_score), axis=-1)  7.17 us
  transfers between devices with their start and end apart: 2, of which 1 were waited for; matrix products, arithmetic and copies ran while one was open for 27% of the time, Pallas kernels for 0%

commit v1 on v0

--- a/solution.py
+++ b/solution.py
@@ -11,6 +11,18 @@
 ROPE_BASE = 10000.0
 norm_eps = 1e-06
 masked_score = -1000000000.0
+
+
+def _register_rails(my_tile, axis_id="tp"):
+    return jnp.concatenate(
+        lax.all_to_all(
+            jnp.stack(jnp.split(my_tile, lax.axis_size(axis_id), axis=0)),
+            axis_name=axis_id,
+            split_axis=0,
+            concat_axis=0,
+        ),
+        axis=1,
+    )
 
 
 def copy_for_each(x, axis):
@@ -215,7 +227,7 @@
         .reshape(tok_rows, heads_local * HEAD_DIM)
         .astype(jnp.bfloat16)
     )
-    head_rows = lax.all_to_all(mixed, "tp", split_axis=0, concat_axis=1, tiled=True)
+    head_rows = _register_rails(mixed)
     return jnp.dot(head_rows, out_weight, preferred_element_type=jnp.float32).astype(jnp.bfloat16)
 
 

time: 173 us -> 167 us (0.965)
  local copies, waits for them, and re-layouts: 44 us -> 35.9 us
  other arithmetic: 27.4 us -> 24.6 us
  waiting for transfers between devices: 29.5 us -> 32.1 us
  matrix products: 39.3 us -> 41.1 us
    all_to_all x1, waiting for transfers between devices: 29.5 us -> 32.1 us  [per_device(): lax.all_to_all(outgoing, 'kv', split_axis=1, concat_axis=1, tiled=True)]
    another operation x1, local copies, waits for them, and re-layouts: 2.51 us -> 0.01 us  [_register_rails(): jnp.stack(jnp.split(my_tile, lax.axis_size(axis_id), axis=0))]
    concatenate x6, local copies, waits for them, and re-layouts: 2.81 us -> 0.74 us  [rotate(): jnp.concatenate([first_half * cosine - second_half * sine, second_half *...]
    dot_general x1, matrix products: 9.4 us -> 11.3 us  [per_device(): jnp.einsum('ktgc,kcd->ktgd', cmp_probs.astype(jnp.bfloat16), summaries[.....]
    unnamed x58 -> x57, local copies, waits for them, and re-layouts: 10.2 us -> 8.6 us
  transfers between devices with their start and end apart: 2 -> 2, of which waited for: 1 -> 1; matrix products, arithmetic and copies ran while one was open for 27% -> 26% of each run, Pallas kernels for 0% -> 0%
where the time goes in v1:
time: 167 us; the launch traced here: 166 us
  matrix products  41.1 us (25%)
  local copies, waits for them, and re-layouts  35.9 us (21%)
  waiting for transfers between devices  32.1 us (19%)
  other arithmetic  24.6 us (15%)
  blocking collectives  16 us (10%)
  starting transfers between devices  15.3 us (9%)
    all_to_all x1, waiting for transfers between devices, per_device(): lax.all_to_all(outgoing, 'kv', split_axis=1, concat_axis=1, tiled=True)  32.1 us
    all_to_all x1, blocking collectives, _register_rails(): lax.all_to_all(jnp.stack(jnp.split(my_tile, lax.axis_size(axis_id), axis=...  16 us
    dot_general x1, matrix products, per_device(): jnp.einsum('ktgc,kcd->ktgd', cmp_probs.astype(jnp.bfloat16), summaries[.....  11.3 us
    sub x1, matrix products, per_device(): jax.nn.softmax(jnp.where(usable, cmp_scores, masked_score), axis=-1)  10.7 us
    dot_general x1, matrix products, per_device(): jnp.dot(normed, joined_weight, preferred_element_type=jnp.float32)  9.37 us
    unnamed x57, local copies, waits for them, and re-layouts  8.6 us
    all_to_all x1, starting transfers between devices, copy_for_each(): lax.all_to_all(jnp.broadcast_to(x[None], (peers, *x.shape)), axis, 0, 0,...  8.48 us
    sub x1, other arithmetic, per_device(): jax.nn.softmax(jnp.where(allowed_keys, sel_scores, masked_score), axis=-1)  7.14 us
  transfers between devices with their start and end apart: 2, of which 1 were waited for; matrix products, arithmetic and copies ran while one was open for 26% of the time, Pallas kernels for 0%

profile of v1, /device:TPU:1, one launch (start us, length us, event | category | flops | bytes accessed | tf_op | source)
XLA Modules:
  0.0 165.6 jit_solution(8321500910990705629)
XLA Ops:
  0.8 5.1 %fusion.2 = f32[2048]{0:T(1024)S(1)} fusion(bf16[2048,2048]{1,0:T(8,128)(2,1)} %param.16), kind=kLoop, calls=%fused_computation.6 | loop fusion | flops 12580864 | bytes 8396800 | tf_op jit(solution)/shard_map/reduce_sum | solution.py:106
  6.0 0.8 dynamic-slice_bitcast_fusion
  7.4 1.0 copy.57
  8.4 1.0 copy.58
  9.5 1.0 copy.59
  10.5 1.0 copy.60
  12.4 5.5 %concatenate.68 = bf16[2048,388]{1,0:T(8,128)(2,1)} concatenate(bf16[2048,128]{1,0:T(8,128)(2,1)} %param.18, bf16[2048,64]{1,0:T(8,128)(2,1)} %copy.57, bf16[2048,64]{1,0:T(8,128)(2,1)} %copy.58, bf16[2048,64]{1,0:T(8,128)(2,1)} %copy.59, bf16[2048,64]{1,0:T(8,128)(2,1)} %copy.60, bf16[2048,2]{1,0:T(8,128)(2,1)S(1)} %copy.61, bf16[2048,2]{1,0:T(8,128)(2,1)S(1)} %copy.62), dimensions={1} | concatenate | bytes 3178496 | tf_op jit(solution)/shard_map/concatenate | solution.py:114
  17.9 9.4 %fusion.127 = (bf16[2048,388]{0,1:T(8,128)(2,1)S(1)}, f32[2048,388]{0,1:T(8,128)}) fusion(bf16[2048,388]{1,0:T(8,128)(2,1)} %concatenate.68, bf16[2048,2048]{1,0:T(8,128)(2,1)} %param.16, f32[2048]{0:T(1024)S(1)} %convert_element_type.125, f32[2048]{0:T(1024)S(1)} %add_rsqrt_fusion), kind=kOutput, calls=%fused_computation.195 | convolution fusion | flops 3272351744 | bytes 14761984 | tf_op jit(solution)/shard_map/dot_general | solution.py:126
  27.4 1.0 copy-done.9
  31.5 8.5 %all-to-all-start = ((bf16[16,1,64,128]{3,2,1,0:T(8,128)(2,1)}), bf16[16,1,64,128]{3,2,1,0:T(8,128)(2,1)}, u32[]{:S(2)}, u32[]{:S(2)}) async-start(bf16[16,1,64,128]{3,2,1,0:T(8,128)(2,1)} %broadcast_in_dim.34), calls=%async_computation | async-start | bytes 524288 | tf_op jit(solution)/shard_map/all_to_all | solution.py:30
  40.2 1.7 %slice_bitcast_fusion.22 = (bf16[8,8,16,128]{3,1,2,0:T(8,128)(2,1)}, bf16[2048,64]{0,1:T(8,128)(2,1)S(1)}) fusion(bf16[2048,388]{0,1:T(8,128)(2,1)} %copy-done.9), kind=kLoop, calls=%fused_computation.192 | loop fusion | bytes 786432
  41.9 1.0 fusion.83
  42.9 1.1 slice_bitcast_fusion.4
  44.0 1.3 split.66
  46.1 1.8 %multiply_cosine_fusion.1 = (f32[2048,32]{0,1:T(8,128)}, f32[2048,32]{0,1:T(8,128)}) fusion(f32[32]{0:T(128)S(1)} %multiply_power_fusion, f32[2048]{0:T(1024)S(1)} %get-tuple-element.30), kind=kLoop, calls=%fused_computation.56 | loop fusion | flops 65536 | bytes 532608 | tf_op jit(solution)/shard_map/cos | solution.py:48
  48.0 1.1 fusion.35
  49.7 1.7 %broadcast_compare_fusion.1 = pred[16,128,640]{2,1,0:T(8,128)(4,1)} fusion(s32[16,128]{1,0:T(8,128)S(1)} %add_add_fusion, s32[16,640]{1,0:T(8,128)S(1)} %add_bitcast_fusion), kind=kLoop, calls=%fused_computation.30 | loop fusion | flops 1310720 | bytes 1359872 | tf_op jit(solution)/shard_map/le | solution.py:216
  51.9 3.1 %gather_fusion = bf16[256,64,128]{2,1,0:T(8,128)(2,1)} fusion(bf16[1,32,64,128]{3,2,1,0:T(8,128)(2,1)S(1)} %pad_maximum_fusion.1, s32[256]{0:T(256)S(1)} %reshape.732), kind=kCustom, calls=%fused_computation | custom fusion | bytes 8390656 | tf_op jit(solution)/shard_map/gather | solution.py:192
  55.2 6.8 %all-to-all-start.1 = ((bf16[1,16,16,64,128]{4,3,2,0,1:T(8,128)(2,1)}), bf16[1,16,16,64,128]{4,3,2,0,1:T(8,128)(2,1)}, u32[]{:S(2)}, u32[]{:S(2)}) async-start(bf16[1,16,16,64,128]{4,3,2,0,1:T(8,128)(2,1)} %bitcast.184), calls=%async_computation.1 | async-start | bytes 8388608 | tf_op jit(solution)/shard_map/all_to_all | solution.py:193
  62.0 2.1 %split.121 = bf16[2048,128]{0,1:T(8,128)(2,1)} slice(f32[2048,388]{0,1:T(8,128)} %get-tuple-element.24), slice={[0:2048], [0:128]} | slice | bytes 1048576 | tf_op jit(solution)/shard_map/split | solution.py:143
  64.7 4.2 %fusion.126 = (f32[2048,1024]{0,1:T(8,128)}, pred[2048,1024]{0,1:T(8,128)(4,1)S(1)}) fusion(s32[2048]{0:T(1024)S(1)} %get-tuple-element.29, s32[1024]{0:T(1024)S(1)} %multiply_add_fusion), kind=kLoop, calls=%fused_computation.194 | loop fusion | flops 4194304 | bytes 10498048 | tf_op jit(solution)/shard_map/convert_element_type | solution.py:175
  68.8 10.7 %fusion.129 = (f32[2048,2]{0,1:T(2,128)S(1)}, f32[2048,2,1024]{0,2,1:T(8,128)}) fusion(pred[2048,1024]{0,1:T(8,128)(4,1)S(1)} %get-tuple-element.20, bf16[2048,2,64]{0,2,1:T(8,128)(2,1)} %bitcast.198, bf16[1,1024,128]{2,1,0:T(8,128)(2,1)} %bitcast.14), kind=kOutput, calls=%fused_computation.197 | convolution fusion | flops 553649152 | bytes 19677184 | tf_op jit(solution)/shard_map/sub | solution.py:173
  79.5 11.3 %fusion.19 = f32[2048,2,64]{0,2,1:T(8,128)} fusion(f32[2048,2,1024]{0,2,1:T(8,128)} %get-tuple-element.28, f32[2048,1024]{0,1:T(8,128)} %get-tuple-element.19, f32[2048,2]{0,1:T(2,128)S(1)} %get-tuple-element.27, f32[2048,2]{0,1:T(2,128)S(1)} %get-tuple-element.8, bf16[1,1024,128]{2,1,0:T(8,128)(2,1)} %bitcast.14), kind=kOutput, calls=%fused_computation.32 | convolution fusion | flops 549715968 | bytes 26509312 | tf_op jit(solution)/shard_map/ktgc,kcd->ktgd/dot_general | solution.py:176
  90.8 32.1 %all-to-all-done.1 = bf16[1,16,16,64,128]{4,3,2,0,1:T(8,128)(2,1)} async-done(((bf16[1,16,16,64,128]{4,3,2,0,1:T(8,128)(2,1)}), bf16[1,16,16,64,128]{4,3,2,0,1:T(8,128)(2,1)}, u32[]{:S(2)}, u32[]{:S(2)}) %all-to-all-start.1) | async-done | bytes 4194336 | tf_op jit(solution)/shard_map/all_to_all | solution.py:193
  122.9 4.5 %gather_fusion.1 = bf16[128,64,128]{2,1,0:T(8,128)(2,1)} fusion(bf16[1,16,16,64,128]{4,3,2,1,0:T(8,128)(2,1)} %bitcast.31, s32[128]{0:T(128)S(1)} %reshape.740), kind=kCustom, calls=%fused_computation.1 | custom fusion | bytes 4195840 | tf_op jit(solution)/shard_map/gather | solution.py:196
  127.3 2.9 %copy.82 = bf16[1,16,512,128]{2,3,1,0:T(8,128)(2,1)S(1)} copy(bf16[1,16,512,128]{3,2,1,0:T(8,128)(2,1)} %bitcast.185) | data formatting | bytes 4194304 | tf_op jit(solution)/shard_map/reshape | solution.py:199
  130.6 1.6 copy-done.2
  132.1 1.6 fusion.22
  133.7 7.1 %fusion.128 = (f32[16,128,2]{1,2,0:T(2,128)S(1)}, f32[16,128,2,640]{3,1,2,0:T(8,128)}) fusion(f32[16,128,2,640]{3,1,2,0:T(8,128)S(1)} %fusion.22, pred[16,128,640]{2,1,0:T(8,128)(4,1)S(1)} %copy-done.4), kind=kOutput, calls=%fused_computation.196 | output fusion | flops 15729279 | bytes 22298624 | tf_op jit(solution)/shard_map/sub | solution.py:217
  140.9 5.2 %fusion.18 = f32[16,128,2,64]{1,3,2,0:T(8,128)S(1)} fusion(f32[16,128,2,640]{3,1,2,0:T(8,128)} %get-tuple-element.26, f32[16,128,2]{1,2,0:T(2,128)S(1)} %get-tuple-element.25, bf16[1,16,640,128]{2,3,1,0:T(8,128)(2,1)S(1)} %copy-done.3), kind=kOutput, calls=%fused_computation.27 | convolution fusion | flops 340787200 | bytes 12861440 | tf_op jit(solution)/shard_map/knqgm,knmd->knqgd/dot_general | solution.py:218
  147.3 16.0 %all_to_all.15 = bf16[8,256,128]{1,2,0:T(8,128)(2,1)S(1)} all-to-all(bf16[8,256,128]{1,2,0:T(8,128)(2,1)S(1)} %fusion.45), channel_id=1, replica_groups=mesh['kv'=16,'tp'=8] {'tp'}, dimensions={0} | all-to-all | bytes 1048576 | tf_op jit(solution)/shard_map/all_to_all | solution.py:18
  163.3 2.3 %convolution_convert_fusion = bf16[256,2048]{1,0:T(8,128)(2,1)} fusion(bf16[256,1024]{0,1:T(8,128)(2,1)S(1)} %bitcast.199, bf16[1024,2048]{1,0:T(8,128)(2,1)S(1)} %copy-done.20), kind=kOutput, calls=%fused_computation.31 | convolution fusion | flops 1074266112 | bytes 5767168 | tf_op jit(solution)/shard_map/dot_general | solution.py:231
  (111 shorter events, 9.6 us)
Async XLA Ops:
  0.0 29.9 %copy-start = (bf16[1,2048,64]{1,2,0:T(8,128)(2,1)S(1)}, bf16[1,2048,64]{1,2,0:T(8,128)(2,1)}, u32[]{:S(2)}) copy-start(bf16[1,2048,64]{1,2,0:T(8,128)(2,1)} %param.25) | copy-start | bytes 786436
  0.0 5.9 %copy-start.18 = (bf16[1,32,64]{2,1,0:T(8,128)(2,1)S(1)}, bf16[1,32,64]{2,1,0:T(8,128)(2,1)}, u32[]{:S(2)}) copy-start(bf16[1,32,64]{2,1,0:T(8,128)(2,1)} %param.24) | copy-start | bytes 12292
  0.0 6.0 %copy-start.19 = (bf16[1,32,64]{2,1,0:T(8,128)(2,1)S(1)}, bf16[1,32,64]{2,1,0:T(8,128)(2,1)}, u32[]{:S(2)}) copy-start(bf16[1,32,64]{2,1,0:T(8,128)(2,1)} %param.27) | copy-start | bytes 12292
  0.0 7.4 %copy-start.10 = (bf16[2048,64]{0,1:T(8,128)(2,1)S(1)}, bf16[2048,64]{0,1:T(8,128)(2,1)}, u32[]{:S(2)}) copy-start(bf16[2048,64]{0,1:T(8,128)(2,1)} %param.19) | copy-start | bytes 786436
  0.0 8.4 %copy-start.11 = (bf16[2048,64]{0,1:T(8,128)(2,1)S(1)}, bf16[2048,64]{0,1:T(8,128)(2,1)}, u32[]{:S(2)}) copy-start(bf16[2048,64]{0,1:T(8,128)(2,1)} %param.20) | copy-start | bytes 786436
  0.8 8.7 %copy-start.12 = (bf16[2048,64]{0,1:T(8,128)(2,1)S(1)}, bf16[2048,64]{0,1:T(8,128)(2,1)}, u32[]{:S(2)}) copy-start(bf16[2048,64]{0,1:T(8,128)(2,1)} %param.21) | copy-start | bytes 786436
  0.8 9.7 %copy-start.13 = (bf16[2048,64]{0,1:T(8,128)(2,1)S(1)}, bf16[2048,64]{0,1:T(8,128)(2,1)}, u32[]{:S(2)}) copy-start(bf16[2048,64]{0,1:T(8,128)(2,1)} %param.22) | copy-start | bytes 786436
  27.2 1.2 copy-start.9
  27.2 2.7 %copy-start.16 = (bf16[1,64,64]{2,1,0:T(8,128)(2,1)S(1)}, bf16[1,64,64]{2,1,0:T(8,128)(2,1)}, u32[]{:S(2)}) copy-start(bf16[1,64,64]{2,1,0:T(8,128)(2,1)} %param.26) | copy-start | bytes 24580
  27.2 3.0 %copy-start.14 = (bf16[1,2048,64]{1,2,0:T(8,128)(2,1)S(1)}, bf16[1,2048,64]{1,2,0:T(8,128)(2,1)}, u32[]{:S(2)}) copy-start(bf16[1,2048,64]{1,2,0:T(8,128)(2,1)} %param.28) | copy-start | bytes 786436
  27.2 3.0 %copy-start.17 = (bf16[1,64,64]{2,1,0:T(8,128)(2,1)S(1)}, bf16[1,64,64]{2,1,0:T(8,128)(2,1)}, u32[]{:S(2)}) copy-start(bf16[1,64,64]{2,1,0:T(8,128)(2,1)} %param.29) | copy-start | bytes 24580
  27.2 12.8 %copy-start.15 = (s32[1,256,8]{1,2,0:T(8,128)S(1)}, s32[1,256,8]{1,2,0:T(8,128)}, u32[]{:S(2)}) copy-start(s32[1,256,8]{1,2,0:T(8,128)} %param.31) | copy-start | bytes 24580
  31.5 23.7 %all-to-all-start = ((bf16[16,1,64,128]{3,2,1,0:T(8,128)(2,1)}), bf16[16,1,64,128]{3,2,1,0:T(8,128)(2,1)}, u32[]{:S(2)}, u32[]{:S(2)}) async-start(bf16[16,1,64,128]{3,2,1,0:T(8,128)(2,1)} %broadcast_in_dim.34), calls=%async_computation | async-start | bytes 524288 | tf_op jit(solution)/shard_map/all_to_all | solution.py:30
  51.9 3.1 %copy-start.7 = (f32[2048,32]{0,1:T(8,128)S(1)}, f32[2048,32]{0,1:T(8,128)}, u32[]{:S(2)}) copy-start(f32[2048,32]{0,1:T(8,128)} %get-tuple-element.21) | copy-start | bytes 786436
  51.9 3.1 %copy-start.8 = (f32[2048,32]{0,1:T(8,128)S(1)}, f32[2048,32]{0,1:T(8,128)}, u32[]{:S(2)}) copy-start(f32[2048,32]{0,1:T(8,128)} %get-tuple-element.22) | copy-start | bytes 786436
  55.2 9.1 %copy-start.5 = (bf16[8,8,16,128]{3,1,2,0:T(8,128)(2,1)S(1)}, bf16[8,8,16,128]{3,1,2,0:T(8,128)(2,1)}, u32[]{:S(2)}) copy-start(bf16[8,8,16,128]{3,1,2,0:T(8,128)(2,1)} %get-tuple-element.11) | copy-start | bytes 786436
  55.2 67.7 %all-to-all-start.1 = ((bf16[1,16,16,64,128]{4,3,2,0,1:T(8,128)(2,1)}), bf16[1,16,16,64,128]{4,3,2,0,1:T(8,128)(2,1)}, u32[]{:S(2)}, u32[]{:S(2)}) async-start(bf16[1,16,16,64,128]{4,3,2,0,1:T(8,128)(2,1)} %bitcast.184), calls=%async_computation.1 | async-start | bytes 8388608 | tf_op jit(solution)/shard_map/all_to_all | solution.py:193
  130.6 1.6 copy-start.2
  132.1 1.6 copy-start.4
  133.7 7.2 %copy-start.3 = (bf16[1,16,640,128]{2,3,1,0:T(8,128)(2,1)S(1)}, bf16[1,16,640,128]{2,3,1,0:T(8,128)(2,1)}, u32[]{:S(2)}) copy-start(bf16[1,16,640,128]{2,3,1,0:T(8,128)(2,1)} %copy-done.2) | copy-start | bytes 7864324
  140.9 5.9 %copy-start.6 = (f32[2048,2,64]{0,2,1:T(8,128)S(1)}, f32[2048,2,64]{0,2,1:T(8,128)}, u32[]{:S(2)}) copy-start(f32[2048,2,64]{0,2,1:T(8,128)} %fusion.19) | copy-start | bytes 3145732
  146.1 17.2 %copy-start.20 = (bf16[1024,2048]{1,0:T(8,128)(2,1)S(1)}, bf16[1024,2048]{1,0:T(8,128)(2,1)}, u32[]{:S(2)}) copy-start(bf16[1024,2048]{1,0:T(8,128)(2,1)} %param.30) | copy-start | bytes 12582916
  146.7 18.9 %copy-start.1 = (bf16[1,2048,64]{1,2,0:T(8,128)(2,1)S(1)}, bf16[1,2048,64]{1,2,0:T(8,128)(2,1)}, u32[]{:S(2)}) copy-start(bf16[1,2048,64]{1,2,0:T(8,128)(2,1)} %param.25) | copy-start | bytes 786436
